TPU v7x, 256 devices: a whole 4x4x8 slice. The times are simulated.
256 devices in a mesh: ep: 32 (over z, x), tp: 8 (over y, core).
Axes of the slice: x: 4, y: 4, z: 8, core: 2. Of those that a mesh axis runs over, the one named last changes fastest.
Arguments:
- tokens: bfloat16 [8192, 2048], P('ep'), may hold values from -6 to 6
- routes: int32 [8192, 2], P('ep'), may hold values from 0 to 31, all different within a row; in each aligned block of 256 rows (0 to 255, 256 to 511, ...) at most 32 rows name the same one
- router_matrix: bfloat16 [2048, 32], replicated, may hold values from -0.125 to 0.125
- cotangent: bfloat16 [8192, 2048], P('ep', 'tp'), may hold values from -3 to 3
- gate_proj: bfloat16 [32, 2048, 3584], P('ep', None, 'tp'), may hold values from -0.125 to 0.125
- up_proj: bfloat16 [32, 2048, 3584], P('ep', None, 'tp'), may hold values from -0.125 to 0.125
- down_proj: bfloat16 [32, 3584, 2048], P('ep', 'tp'), may hold values from -0.09375 to 0.09375
Outputs:
- token_grad: bfloat16 [8192, 2048], P('ep', 'tp')
- mixing_grad: float32 [8192, 2], P('ep')
- router_grad: float32 [2048, 32], P(('ep', 'tp'))
- gate_grad: bfloat16 [32, 2048, 3584], P('ep', None, 'tp')
- up_grad: bfloat16 [32, 2048, 3584], P('ep', None, 'tp')
- down_grad: bfloat16 [32, 3584, 2048], P('ep', 'tp')
Inputs may be any that keep to these rules, and one draw needn't show every extreme that they name: `routes`: the two experts of a row differ. In each aligned block of 256 rows no expert is named by more than 32 rows, a bound that some block reaches; every expert is named somewhere.
All inputs are finite; a program needn't handle non-finite values.
Results may differ from a plain program's by a relative error of at most 0.019.
Values may be sent and summed in bfloat16 or wider, within the bound.
A program may use at most 128 MiB of HBM per device.

v0:
```python
import math

import jax
import jax.numpy as jnp
from jax import lax
from jax.sharding import PartitionSpec as P


def side_by_side(arrays, axis, split_dim, concat_dim, along):
    widths = [math.prod(a.shape[along:]) for a in arrays]
    both = jnp.concatenate(
        [a.reshape(*a.shape[:along], w) for a, w in zip(arrays, widths)], axis=along
    )
    whole = lax.all_to_all(both, axis, split_axis=split_dim, concat_axis=concat_dim, tiled=True)
    pieces = jnp.split(whole, [sum(widths[:k]) for k in range(1, len(widths))], axis=along)
    return tuple(
        (b.reshape(*whole.shape[:along], *a.shape[along:]) for a, b in zip(arrays, pieces))
    )


def side_by_side_2(arrays, axis, dim, along):
    both = jnp.concatenate(arrays, axis=along)
    whole, at, done = (lax.all_gather(both, axis, axis=dim, tiled=True), 0, [])
    for a in arrays:
        done.append(lax.slice_in_dim(whole, at, at + a.shape[along], axis=along))
        at += a.shape[along]
    return tuple(done)


def sent_to_all(shard, axis):
    copies = jnp.broadcast_to(shard, (lax.axis_size(axis), *shard.shape))
    return lax.all_to_all(copies, axis, split_axis=0, concat_axis=0, tiled=True)


def over_copies(shard, axis):
    everything = sent_to_all(shard, axis)
    return jnp.sum(everything, axis=0)


def split_up(shard, dim, length):
    shape = shard.shape
    pieces = shard.reshape(*shape[:dim], length, shape[dim] // length, *shape[dim + 1 :])
    return jnp.moveaxis(pieces, dim, 0)


def sum_at_owner(shard, axis, dim):
    pieces = split_up(shard, dim, lax.axis_size(axis))
    arrived = lax.all_to_all(pieces, axis, split_axis=0, concat_axis=0, tiled=True)
    return arrived.astype(jnp.float32).sum(axis=0)


def slot_places(flat_routes, experts, capacity):
    onehot = (flat_routes[:, None] == jnp.arange(experts, dtype=jnp.int32)[None, :]).astype(
        jnp.int32
    )
    earlier = jnp.cumsum(onehot, axis=0) - onehot
    places = flat_routes * capacity + jnp.sum(earlier * onehot, axis=1)
    entries = flat_routes.shape[0]
    filler = (
        jnp.full((experts * capacity,), entries, jnp.int32)
        .at[places]
        .set(jnp.arange(entries, dtype=jnp.int32))
    )
    return (places, filler)


def local(tokens, routes, router_matrix, cotangent, gate_proj, up_proj, down_proj):
    ep_size = lax.axis_size("ep")
    tp_size = lax.axis_size("tp")
    tp_index = lax.axis_index("tp")
    home_rows, model_width = tokens.shape
    top_count = routes.shape[1]
    experts = router_matrix.shape[1]
    capacity = home_rows * top_count * 2 // experts
    entries = home_rows * top_count
    col_width = model_width // tp_size
    places, filler = slot_places(routes.reshape(-1), experts, capacity)
    occupied = filler < entries
    source = jnp.where(occupied, filler // top_count, 0)
    entry_src = jnp.where(occupied, filler, 0)
    logits = jnp.dot(tokens, router_matrix, preferred_element_type=jnp.float32)
    picked = routes[:, :, None] == jnp.arange(experts, dtype=jnp.int32)[None, None, :]
    chosen = jnp.sum(jnp.where(picked, logits[:, None, :], 0.0), axis=2)
    mixing = jax.nn.sigmoid(chosen - chosen[:, ::-1])
    mix_send = (
        jnp.where(occupied, mixing.reshape(-1)[entry_src], 0.0)
        .astype(jnp.bfloat16)
        .reshape(experts, capacity)
    )
    zero_value = jnp.zeros((), jnp.bfloat16)
    token_cols = lax.dynamic_slice_in_dim(tokens, tp_index * col_width, col_width, 1)
    token_send = jnp.where(occupied[:, None], token_cols[source], zero_value).reshape(
        experts, capacity, col_width
    )
    output_send = jnp.where(occupied[:, None], cotangent[source], zero_value).reshape(
        experts, capacity, col_width
    )
    token_part_in, output_part_in, mix_in = side_by_side(
        (token_send, output_send, mix_send), "ep", 0, 0, 2
    )
    token_in, output_in = side_by_side_2((token_part_in, output_part_in), "tp", 2, 0)
    senders = token_in.shape[0]
    slots = senders * capacity
    token_rows = token_in.reshape(slots, model_width)
    output_rows = output_in.reshape(slots, model_width)
    mix_value = mix_in.reshape(slots).astype(jnp.float32)
    w_gate = gate_proj[0]
    w_up = up_proj[0]
    w_down = down_proj[0]
    over_rows = (((0,), (0,)), ((), ()))
    over_cols = (((1,), (1,)), ((), ()))
    gate_pre = jnp.dot(token_rows, w_gate, preferred_element_type=jnp.float32)
    up_pre = jnp.dot(token_rows, w_up, preferred_element_type=jnp.float32)
    gate_sig = jax.nn.sigmoid(gate_pre)
    active = gate_pre * gate_sig
    hidden = (active * up_pre).astype(jnp.bfloat16)
    back_hidden = lax.dot_general(
        output_rows, w_down, over_cols, preferred_element_type=jnp.float32
    )
    mix_part = jnp.sum(hidden.astype(jnp.float32) * back_hidden, axis=1)
    scaled = mix_value[:, None] * back_hidden
    gate_back = (scaled * up_pre * gate_sig * (1.0 + gate_pre * (1.0 - gate_sig))).astype(
        jnp.bfloat16
    )
    up_back = (scaled * active).astype(jnp.bfloat16)
    out_scaled = (mix_value[:, None] * output_rows).astype(jnp.bfloat16)
    gate_grad = lax.dot_general(
        token_rows, gate_back, over_rows, preferred_element_type=jnp.float32
    ).astype(jnp.bfloat16)[None]
    up_grad = lax.dot_general(
        token_rows, up_back, over_rows, preferred_element_type=jnp.float32
    ).astype(jnp.bfloat16)[None]
    down_grad = lax.dot_general(
        hidden, out_scaled, over_rows, preferred_element_type=jnp.float32
    ).astype(jnp.bfloat16)[None]
    slot_terms = lax.dot_general(gate_back, w_gate, over_cols, preferred_element_type=jnp.float32)
    slot_terms = slot_terms + lax.dot_general(
        up_back, w_up, over_cols, preferred_element_type=jnp.float32
    )
    summed = lax.psum_scatter(
        slot_terms.reshape(senders, capacity, model_width).astype(jnp.bfloat16),
        "tp",
        scatter_dimension=2,
        tiled=True,
    )
    mix_total = over_copies(mix_part.reshape(senders, capacity), "tp")
    back_rows = lax.all_to_all(summed, "ep", split_axis=0, concat_axis=0, tiled=True)
    back_mix = lax.all_to_all(mix_total, "ep", split_axis=0, concat_axis=0, tiled=True)
    back_flat = back_rows.reshape(experts * capacity, col_width)
    token_part = jnp.sum(
        back_flat[places].reshape(home_rows, top_count, col_width).astype(jnp.float32), axis=1
    )
    mixing_grad = back_mix.reshape(-1)[places].reshape(home_rows, top_count)
    pairwise = mixing[:, 0] * mixing[:, 1]
    logit_grad = pairwise[:, None] * (mixing_grad - mixing_grad[:, ::-1])
    route_grad = jnp.sum(jnp.where(picked, logit_grad[:, :, None], 0.0), axis=1)
    router_cols = lax.dynamic_slice_in_dim(
        router_matrix, tp_index * col_width, col_width, 0
    ).astype(jnp.float32)
    router_path = jnp.dot(route_grad, router_cols.T)
    token_grad = (token_part + router_path).astype(jnp.bfloat16)
    row_share = model_width // (ep_size * tp_size)
    feature_share = lax.dynamic_slice_in_dim(
        tokens.reshape(home_rows, ep_size, tp_size, row_share), tp_index, 1, 2
    )
    feature_share = feature_share.reshape(home_rows, ep_size * row_share).astype(jnp.float32)
    norm_scale = 1.0 / math.sqrt(home_rows * ep_size)
    router_grad = sum_at_owner(
        (jnp.dot(feature_share.T, route_grad) * norm_scale).astype(jnp.bfloat16), "ep", 0
    )
    return (token_grad, mixing_grad, router_grad, gate_grad, up_grad, down_grad)


def solution(mesh):
    return jax.shard_map(
        local,
        mesh=mesh,
        in_specs=(
            P("ep", None),
            P("ep", None),
            P(),
            P("ep", "tp"),
            P("ep", None, "tp"),
            P("ep", None, "tp"),
            P("ep", "tp", None),
        ),
        out_specs=(
            P("ep", "tp"),
            P("ep", None),
            P(("ep", "tp"), None),
            P("ep", None, "tp"),
            P("ep", None, "tp"),
            P("ep", "tp", None),
        ),
        check_vma=False,
    )
```

profile of v0, /device:TPU:8, one launch (start us, length us, event | category | flops | bytes accessed | tf_op | source)
XLA Modules:
  0.0 234.9 jit_solution(10823893233557745330)
XLA Ops:
  11.0 2.4 %scatter_custom_fusion = s32[1024]{0:T(1024)S(1)} fusion(s32[512]{0:T(512)S(1)} %bitcast.84, s32[512]{0:T(512)S(1)} %iota.15, s32[]{:T(128)} %constant.14.clone.1), kind=kCustom, calls=%fused_computation.74 | custom fusion | bytes 4100 | tf_op jit(solution)/shard_map/scatter | solution.py:62
  15.7 6.8 %gather_fusion.2 = bf16[1024]{0:T(1024)(128)(2,1)S(1)} fusion(bf16[512]{0:T(512)(128)(2,1)S(1)} %reshape.121, s32[1024]{0:T(1024)S(1)} %fusion.28), kind=kCustom, calls=%fused_computation.2 | custom fusion | bytes 8192 | tf_op jit(solution)/shard_map/gather | solution.py:86
  23.9 3.9 %gather_fusion = bf16[1024,256]{1,0:T(8,128)(2,1)S(1)} fusion(bf16[256,256]{1,0:T(8,128)(2,1)S(1)} %constant_dynamic-slice_fusion, s32[1024]{0:T(1024)S(1)} %get-tuple-element.32), kind=kCustom, calls=%fused_computation | custom fusion | bytes 1052672 | tf_op jit(solution)/shard_map/gather | solution.py:92
  27.9 3.9 %gather_fusion.1 = bf16[1024,256]{1,0:T(8,128)(2,1)S(1)} fusion(bf16[256,256]{1,0:T(8,128)(2,1)S(1)} %copy-done.1, s32[1024]{0:T(1024)S(1)} %get-tuple-element.32), kind=kCustom, calls=%fused_computation.1 | custom fusion | bytes 1052672 | tf_op jit(solution)/shard_map/gather | solution.py:95
  32.1 46.4 %all_to_all.29 = bf16[32,32,513]{2,1,0:T(8,128)(2,1)S(1)} all-to-all(bf16[32,32,513]{2,1,0:T(8,128)(2,1)S(1)} %pad_maximum_fusion), channel_id=1, replica_groups=mesh['ep'=32,'tp'=8] {'ep'}, dimensions={0} | all-to-all | bytes 2101248 | tf_op jit(solution)/shard_map/all_to_all | solution.py:14
  80.2 51.2 %all-gather.2.cloned.1.call-done = bf16[64,32,2048]{2,1,0:T(8,128)(2,1)} async-done(((bf16[64,32,256]{2,1,0:T(8,128)(2,1)}), bf16[64,32,2048]{2,1,0:T(8,128)(2,1)}) %all-gather.2.cloned.1.call-update) | async-done | bytes 8388624 | tf_op jit(solution)/shard_map/all_gather | solution.py:23
  131.4 3.8 %fusion.34 = (bf16[32,32,2048]{2,1,0:T(8,128)(2,1)S(1)}, bf16[32,32,2048]{2,1,0:T(8,128)(2,1)S(1)}) fusion(bf16[64,32,2048]{2,1,0:T(8,128)(2,1)} %all-gather.2.cloned.1.call-done), kind=kLoop, calls=%fused_computation.81 | loop fusion | bytes 16777216 | tf_op jit(solution)/shard_map/slice | solution.py:25
  135.3 2.1 fusion.8
  138.2 2.1 fusion.11
  140.3 3.9 %multiply_reduce_fusion = (f32[1024]{0:T(1024)S(1)}, bf16[1024,448]{0,1:T(8,128)(2,1)}, bf16[1024,448]{0,1:T(8,128)(2,1)S(1)}, bf16[1024,448]{0,1:T(8,128)(2,1)S(1)}) fusion(f32[1024,448]{0,1:T(8,128)S(1)} %fusion.11, f32[1024,448]{0,1:T(8,128)S(1)} %fusion.8, f32[1024]{0:T(1024)S(1)} %reshape.131, bf16[1024,2048]{1,0:T(8,128)(2,1)S(1)} %bitcast.74, ...), kind=kOutput, calls=%fused_computation.25 | convolution fusion | flops 1887763456 | bytes 12460032 | tf_op jit(solution)/shard_map/dot_general | solution.py:117
  144.2 2.4 %fusion.6 = f32[1024,2048]{1,0:T(8,128)S(1)} fusion(bf16[1024,448]{0,1:T(8,128)(2,1)S(1)} %get-tuple-element.36, bf16[1,2048,448]{1,2,0:T(8,128)(2,1)S(1)} %copy-done), kind=kOutput, calls=%fused_computation.16 | convolution fusion | flops 1879048192 | bytes 11141120 | tf_op jit(solution)/shard_map/dot_general | solution.py:136
  146.6 4.4 %add_convert_fusion = bf16[1024,2048]{1,0:T(8,128)(2,1)} fusion(f32[1024,2048]{1,0:T(8,128)S(1)} %fusion.6, bf16[1024,448]{0,1:T(8,128)(2,1)S(1)} %get-tuple-element.37, bf16[1,2048,448]{1,2,0:T(8,128)(2,1)S(1)} %copy-done.8), kind=kOutput, calls=%fused_computation.7 | convolution fusion | flops 1883242496 | bytes 15335424 | tf_op jit(solution)/shard_map/dot_general | solution.py:137
  151.8 4.5 %all-to-all-start.2 = ((f32[8,1,1024]{2,1,0:T(1,128)}), f32[8,1,1024]{2,1,0:T(1,128)S(1)}, u32[]{:S(2)}, u32[]{:S(2)}) async-start(f32[8,1,1024]{2,1,0:T(1,128)} %reshape.197), calls=%async_computation.3 | async-start | bytes 65536 | tf_op jit(solution)/shard_map/all_to_all | solution.py:32
  156.3 4.0 %all-to-all-done.2 = f32[8,1,1024]{2,1,0:T(1,128)S(1)} async-done(((f32[8,1,1024]{2,1,0:T(1,128)}), f32[8,1,1024]{2,1,0:T(1,128)S(1)}, u32[]{:S(2)}, u32[]{:S(2)}) %all-to-all-start.2) | async-done | bytes 32800 | tf_op jit(solution)/shard_map/all_to_all | solution.py:32
  162.3 10.0 %all-to-all-start.3 = ((f32[32,1,32]{2,1,0:T(1,128)}), f32[32,1,32]{2,1,0:T(1,128)S(1)}, u32[]{:S(2)}, u32[]{:S(2)}) async-start(f32[32,1,32]{2,1,0:T(1,128)} %bitcast.14), calls=%async_computation.4 | async-start | bytes 32768 | tf_op jit(solution)/shard_map/all_to_all | solution.py:148
  173.7 8.1 %all-to-all-done.3 = f32[32,1,32]{2,1,0:T(1,128)S(1)} async-done(((f32[32,1,32]{2,1,0:T(1,128)}), f32[32,1,32]{2,1,0:T(1,128)S(1)}, u32[]{:S(2)}, u32[]{:S(2)}) %all-to-all-start.3) | async-done | bytes 4128 | tf_op jit(solution)/shard_map/all_to_all | solution.py:148
  183.1 2.3 gather_fusion.4
  187.8 3.8 %all-to-all-start.4 = ((bf16[32,2,128]{2,1,0:T(2,128)(2,1)}), bf16[32,2,128]{2,1,0:T(2,128)(2,1)S(1)}, u32[]{:S(2)}, u32[]{:S(2)}) async-start(bf16[32,2,128]{2,1,0:T(2,128)(2,1)} %reshape.199), calls=%async_computation.5 | async-start | bytes 32768 | tf_op jit(solution)/shard_map/all_to_all | solution.py:48
  191.7 5.8 %fusion.4 = bf16[1,2048,448]{1,2,0:T(8,128)(2,1)} fusion(bf16[1024,448]{0,1:T(8,128)(2,1)} %copy-done.9, bf16[1024,2048]{1,0:T(8,128)(2,1)} %bitcast.78), kind=kOutput, calls=%fused_computation.14 | convolution fusion | flops 1879965696 | bytes 6946816 | tf_op jit(solution)/shard_map/dot_general | solution.py:127
  197.5 3.8 %all-to-all-done.4 = bf16[32,2,128]{2,1,0:T(2,128)(2,1)S(1)} async-done(((bf16[32,2,128]{2,1,0:T(2,128)(2,1)}), bf16[32,2,128]{2,1,0:T(2,128)(2,1)S(1)}, u32[]{:S(2)}, u32[]{:S(2)}) %all-to-all-start.4) | async-done | bytes 16416 | tf_op jit(solution)/shard_map/all_to_all | solution.py:48
  201.4 5.9 %all-to-all-start.1 = ((bf16[32,32,256]{2,1,0:T(8,128)(2,1)}), bf16[32,32,256]{2,1,0:T(8,128)(2,1)S(1)}, u32[]{:S(2)}, u32[]{:S(2)}) async-start(bf16[32,32,256]{2,1,0:T(8,128)(2,1)} %reduce-scatter.2.cloned.1.call-done), calls=%async_computation.2 | async-start | bytes 1048576 | tf_op jit(solution)/shard_map/all_to_all | solution.py:147
  207.4 5.6 %fusion.5 = bf16[1,2048,448]{1,2,0:T(8,128)(2,1)} fusion(bf16[1024,448]{0,1:T(8,128)(2,1)S(1)} %copy-done.11, bf16[1024,2048]{1,0:T(8,128)(2,1)} %bitcast.79), kind=kOutput, calls=%fused_computation.15 | convolution fusion | flops 1879965696 | bytes 6946816 | tf_op jit(solution)/shard_map/dot_general | solution.py:130
  213.0 3.4 %fusion.3 = bf16[1,448,2048]{2,1,0:T(8,128)(2,1)} fusion(bf16[1024,448]{0,1:T(8,128)(2,1)S(1)} %copy-done.12, bf16[1024,2048]{1,0:T(8,128)(2,1)S(1)} %bitcast.75, f32[1024]{0:T(1024)S(1)} %reshape.131), kind=kOutput, calls=%fused_computation.13 | convolution fusion | flops 1886257152 | bytes 6950912 | tf_op jit(solution)/shard_map/dot_general | solution.py:133
  217.8 5.8 %all-to-all-done.1 = bf16[32,32,256]{2,1,0:T(8,128)(2,1)S(1)} async-done(((bf16[32,32,256]{2,1,0:T(8,128)(2,1)}), bf16[32,32,256]{2,1,0:T(8,128)(2,1)S(1)}, u32[]{:S(2)}, u32[]{:S(2)}) %all-to-all-start.1) | async-done | bytes 524320 | tf_op jit(solution)/shard_map/all_to_all | solution.py:147
  (91 shorter events, 23.8 us)
Async XLA Ops:
  7.2 128.1 %copy-start = (bf16[1,2048,448]{1,2,0:T(8,128)(2,1)S(1)}, bf16[1,2048,448]{1,2,0:T(8,128)(2,1)}, u32[]{:S(2)}) copy-start(bf16[1,2048,448]{1,2,0:T(8,128)(2,1)} %param.11) | copy-start | bytes 5505028
  7.2 8.1 %copy-start.6 = (s32[256,2]{0,1:T(2,128)S(1)}, s32[256,2]{0,1:T(2,128)}, u32[]{:S(2)}) copy-start(s32[256,2]{0,1:T(2,128)} %param.8) | copy-start | bytes 6148
  7.2 124.2 %all-gather.2.cloned.1.call-start = ((), (), s32[]{:S(2)}) async-start(), calls=%async_computation.6 | async-start | bytes 9437184 | tf_op jit(solution)/shard_map/all_gather | solution.py:23
  23.9 4.0 %copy-start.1 = (bf16[256,256]{1,0:T(8,128)(2,1)S(1)}, bf16[256,256]{1,0:T(8,128)(2,1)}, u32[]{:S(2)}) copy-start(bf16[256,256]{1,0:T(8,128)(2,1)} %param.10) | copy-start | bytes 393220
  79.7 121.6 %reduce-scatter.2.cloned.1.call-start = ((), (), s32[]{:S(2)}) async-start(), calls=%async_computation.7 | async-start | bytes 4718592 | tf_op jit(solution)/shard_map/reduce_scatter | solution.py:140
  135.2 2.1 copy-start.5
  135.2 5.0 %copy-start.3 = (bf16[32,32,2048]{2,1,0:T(8,128)(2,1)}, bf16[32,32,2048]{2,1,0:T(8,128)(2,1)S(1)}, u32[]{:S(2)}) copy-start(bf16[32,32,2048]{2,1,0:T(8,128)(2,1)S(1)} %get-tuple-element.34) | copy-start | bytes 12582916
  135.3 2.9 %copy-start.8 = (bf16[1,2048,448]{1,2,0:T(8,128)(2,1)S(1)}, bf16[1,2048,448]{1,2,0:T(8,128)(2,1)}, u32[]{:S(2)}) copy-start(bf16[1,2048,448]{1,2,0:T(8,128)(2,1)} %param.12) | copy-start | bytes 5505028
  138.1 2.1 copy-start.7
  144.2 2.4 %copy-start.9 = (bf16[1024,448]{0,1:T(8,128)(2,1)}, bf16[1024,448]{0,1:T(8,128)(2,1)S(1)}, u32[]{:S(2)}) copy-start(bf16[1024,448]{0,1:T(8,128)(2,1)S(1)} %get-tuple-element.36) | copy-start | bytes 2752516
  144.2 2.4 %copy-start.10 = (bf16[1024,448]{0,1:T(8,128)(2,1)}, bf16[1024,448]{0,1:T(8,128)(2,1)S(1)}, u32[]{:S(2)}) copy-start(bf16[1024,448]{0,1:T(8,128)(2,1)S(1)} %get-tuple-element.37) | copy-start | bytes 2752516
  150.9 21.4 %copy-start.2 = (bf16[256,2048]{1,0:T(8,128)(2,1)S(1)}, bf16[256,2048]{1,0:T(8,128)(2,1)}, u32[]{:S(2)}) copy-start(bf16[256,2048]{1,0:T(8,128)(2,1)} %param.7) | copy-start | bytes 3145732
  151.8 8.5 %all-to-all-start.2 = ((f32[8,1,1024]{2,1,0:T(1,128)}), f32[8,1,1024]{2,1,0:T(1,128)S(1)}, u32[]{:S(2)}, u32[]{:S(2)}) async-start(f32[8,1,1024]{2,1,0:T(1,128)} %reshape.197), calls=%async_computation.3 | async-start | bytes 65536 | tf_op jit(solution)/shard_map/all_to_all | solution.py:32
  162.3 19.5 %all-to-all-start.3 = ((f32[32,1,32]{2,1,0:T(1,128)}), f32[32,1,32]{2,1,0:T(1,128)S(1)}, u32[]{:S(2)}, u32[]{:S(2)}) async-start(f32[32,1,32]{2,1,0:T(1,128)} %bitcast.14), calls=%async_computation.4 | async-start | bytes 32768 | tf_op jit(solution)/shard_map/all_to_all | solution.py:148
  187.8 13.5 %all-to-all-start.4 = ((bf16[32,2,128]{2,1,0:T(2,128)(2,1)}), bf16[32,2,128]{2,1,0:T(2,128)(2,1)S(1)}, u32[]{:S(2)}, u32[]{:S(2)}) async-start(bf16[32,2,128]{2,1,0:T(2,128)(2,1)} %reshape.199), calls=%async_computation.5 | async-start | bytes 32768 | tf_op jit(solution)/shard_map/all_to_all | solution.py:48
  191.7 15.6 %copy-start.11 = (bf16[1024,448]{0,1:T(8,128)(2,1)S(1)}, bf16[1024,448]{0,1:T(8,128)(2,1)}, u32[]{:S(2)}) copy-start(bf16[1024,448]{0,1:T(8,128)(2,1)} %copy-done.10) | copy-start | bytes 2752516
  201.4 22.2 %all-to-all-start.1 = ((bf16[32,32,256]{2,1,0:T(8,128)(2,1)}), bf16[32,32,256]{2,1,0:T(8,128)(2,1)S(1)}, u32[]{:S(2)}, u32[]{:S(2)}) async-start(bf16[32,32,256]{2,1,0:T(8,128)(2,1)} %reduce-scatter.2.cloned.1.call-done), calls=%async_computation.2 | async-start | bytes 1048576 | tf_op jit(solution)/shard_map/all_to_all | solution.py:147
  207.3 5.7 %copy-start.4 = (bf16[32,32,2048]{2,1,0:T(8,128)(2,1)S(1)}, bf16[32,32,2048]{2,1,0:T(8,128)(2,1)}, u32[]{:S(2)}) copy-start(bf16[32,32,2048]{2,1,0:T(8,128)(2,1)} %copy-done.3) | copy-start | bytes 12582916
  207.3 5.7 %copy-start.12 = (bf16[1024,448]{0,1:T(8,128)(2,1)S(1)}, bf16[1024,448]{0,1:T(8,128)(2,1)}, u32[]{:S(2)}) copy-start(bf16[1024,448]{0,1:T(8,128)(2,1)} %get-tuple-element.31) | copy-start | bytes 2752516
Sparse Core Ops, SparseCore 0:
  79.9 51.5 all-gather.1
  151.1 38.2 reduce-scatter.1
where the time goes:
time: 236 us; the launch traced here: 235 us
  waiting for transfers between devices  73 us (31%)
  blocking collectives  46.4 us (20%)
  local copies, waits for them, and re-layouts  35.2 us (15%)
  matrix products  34.1 us (14%)
  starting transfers between devices  24.6 us (10%)
  between operations  14.5 us (6%)
  other arithmetic  7.21 us (3%)
    all_gather x1, waiting for transfers between devices, side_by_side_2(): whole, at, done = (lax.all_gather(both, axis, axis=dim, tiled=True), 0, [])  51.2 us
    all_to_all x1, blocking collectives, side_by_side(): lax.all_to_all(both, axis, split_axis=split_dim, concat_axis=concat_dim,...  46.4 us
    all_to_all x1, starting transfers between devices, local(): lax.all_to_all(mix_total, 'ep', split_axis=0, concat_axis=0, tiled=True)  10 us
    all_to_all x1, waiting for transfers between devices, local(): lax.all_to_all(mix_total, 'ep', split_axis=0, concat_axis=0, tiled=True)  8.13 us
    gather x1, local copies, waits for them, and re-layouts, local(): mixing.reshape(-1)[entry_src]  6.8 us
    all_to_all x1, starting transfers between devices, local(): lax.all_to_all(summed, 'ep', split_axis=0, concat_axis=0, tiled=True)  5.93 us
    dot_general x1, matrix products, local(): lax.dot_general(token_rows, gate_back, over_rows, preferred_element_type=...  5.84 us
    all_to_all x1, waiting for transfers between devices, local(): lax.all_to_all(summed, 'ep', split_axis=0, concat_axis=0, tiled=True)  5.78 us
  transfers between devices with their start and end apart: 6, of which 5 were waited for; matrix products, arithmetic and copies ran while one was open for 11% of the time, Pallas kernels for 0%

commit v1 on v0

v1 whole, which is shorter than its diff:
```python
import math

import jax
import jax.numpy as jnp
from jax import lax
from jax.experimental import pallas as pl
from jax.experimental.pallas import tpu as pltpu
from jax.sharding import PartitionSpec as P

MESH = pl.DeviceIdType.MESH
BF16 = jnp.bfloat16
F32 = jnp.float32

NX, NY = 4, 4
OVER_ROWS = (((0,), (0,)), ((), ()))
OVER_COLS = (((1,), (1,)), ((), ()))


def dot(a, b, dims=None):
    if dims is None:
        return jnp.dot(a, b, preferred_element_type=F32)
    return lax.dot_general(a, b, dims, preferred_element_type=F32)


def iota(shape, dim):
    return lax.broadcasted_iota(jnp.int32, shape, dim)


def halves(value):
    high = value.astype(BF16)
    return high, (value - high.astype(F32)).astype(BF16)


def kernel(
    n_ep, n_tp,
    tokens_h, routes_ref, router_h, cot_h, gate_h, up_h, down_h,
    token_grad_ref, mixing_ref, router_grad_ref, gate_grad_ref, up_grad_ref, down_grad_ref,
    tok, cot, router, wtmp_g, wtmp_u, w2, wd,
    send, ms_send_buf, two_hot, small, gathered, ms_in,
    pre_g, pre_u, back, hid, hid_t, gu, ms_col, mix_col,
    terms, pair_in, near_a, near_b, far_p, far_m, total, ret_in,
    mix_row, mix_all, mix_tot, mix_in, mix_mat, rparts, rin,
    lsem,
    ms_s, ms_r, a2a_s, a2a_r, up_s, up_r, dn_s, dn_r, two_up_s, two_dn_s, two_r, pr_s, pr_r,
    ra_s, ra_r, rb_s, rb_r, rc_s, rc_r, rd_s, rd_r, re_s, re_r,
    mt_s, mt_r, mx_s, mx_r, rt_s, rt_r, ret_s, ret_r,
):
    nz = n_ep // NX
    rows, width = tok.shape
    experts = router.shape[1]
    cap = rows * 2 * 2 // experts
    cols = width // n_tp
    hidden = wtmp_g.shape[1]
    hpad = wd.shape[0]
    slots = experts * cap
    group = NX * cap
    chunk = 2 * group
    chunks = nz // 2
    ep, tp = lax.axis_index("ep"), lax.axis_index("tp")
    z, x = ep // NX, lax.rem(ep, NX)
    y, core = tp // 2, lax.rem(tp, 2)
    offsets = [0]
    for d in range(1, nz // 2 + 1):
        offsets += [d, -d] if d < nz // 2 else [d]

    def ring(value, step, size):
        return lax.rem(value + (step + size), size)

    def tp_of(step):
        return ring(y, step, NY) * 2 + core

    tp_up, tp_dn, tp_far = tp_of(1), tp_of(-1), tp_of(2)
    partner = y * 2 + (1 - core)

    def rcopy(src, dst, s, r, e, t):
        return pltpu.make_async_remote_copy(
            src_ref=src, dst_ref=dst, send_sem=s, recv_sem=r, device_id=(e, t), device_id_type=MESH
        )

    def wait_in(ref, s, r):
        rcopy(ref, ref, s, r, ep, partner).wait_recv()

    def wait_out(ref, s, r):
        rcopy(ref, ref, s, r, ep, partner).wait_send()

    ep_peers = []
    for g, dz in enumerate(offsets):
        for dx in range(NX):
            if dz or dx:
                ep_peers.append((g, ring(z, -dz, nz), ring(x, dx, NX)))

    barrier = pltpu.get_barrier_semaphore()
    for _, pz, px in ep_peers:
        pl.semaphore_signal(barrier, inc=1, device_id=(pz * NX + px, tp), device_id_type=MESH)
    for d in range(1, n_tp):
        pl.semaphore_signal(barrier, inc=1, device_id=(ep, ring(tp, d, n_tp)), device_id_type=MESH)
    loads = [
        pltpu.make_async_copy(a, b, lsem.at[k])
        for k, (a, b) in enumerate(
            (
                (tokens_h, tok), (router_h, router), (cot_h, cot), (gate_h.at[0], wtmp_g),
                (up_h.at[0], wtmp_u), (down_h.at[0], wd.at[pl.ds(0, hidden)]),
            )
        )
    ]
    for load in loads:
        load.start()
    w2[...] = jnp.zeros_like(w2)
    wd[pl.ds(hidden, hpad - hidden), :] = jnp.zeros((hpad - hidden, width), BF16)
    loads[0].wait()
    loads[1].wait()

    lanes = iota((rows, 128), 1)
    r0, r1 = routes_ref[:, 0:1], routes_ref[:, 1:2]
    oh0, oh1 = r0 == lanes, r1 == lanes
    both = jnp.where(oh0 | oh1, 1.0, 0.0).astype(BF16)
    before = jnp.where(iota((rows, rows), 0) > iota((rows, rows), 1), 1.0, 0.0).astype(BF16)
    earlier = dot(before, both)
    rank0 = jnp.sum(jnp.where(oh0, earlier, 0.0), axis=1, keepdims=True)
    rank1 = jnp.sum(jnp.where(oh1, earlier, 0.0), axis=1, keepdims=True)
    logits = dot(tok[...], router[...])
    lane_e = iota((rows, experts), 1)
    chosen0 = jnp.sum(jnp.where(r0 == lane_e, logits, 0.0), axis=1, keepdims=True)
    chosen1 = jnp.sum(jnp.where(r1 == lane_e, logits, 0.0), axis=1, keepdims=True)
    mix0 = jax.nn.sigmoid(chosen0 - chosen1)
    mix1 = jax.nn.sigmoid(chosen1 - chosen0)
    small[:, 0:1] = rank0
    small[:, 1:2] = rank1
    small[:, 2:3] = mix0
    small[:, 3:4] = mix1
    place0 = r0.astype(F32) * cap + rank0
    place1 = r1.astype(F32) * cap + rank1
    mb0 = mix0.astype(BF16).astype(F32)
    mb1 = mix1.astype(BF16).astype(F32)
    loads[2].wait()
    source = jnp.concatenate(
        [tok[:, pl.ds(pl.multiple_of(tp * cols, cols), cols)], cot[...]], axis=1
    )
    for k in range(slots // 128):
        at = (iota((rows, 128), 1) + k * 128).astype(F32)
        hit0, hit1 = place0 == at, place1 == at
        chosen = jnp.where(hit0 | hit1, 1.0, 0.0).astype(BF16)
        two_hot[:, k * 128 : (k + 1) * 128] = chosen
        ms_send_buf[k] = jnp.sum(
            jnp.where(hit0, mb0, 0.0) + jnp.where(hit1, mb1, 0.0), axis=0, keepdims=True
        )
        picked = dot(chosen, source, OVER_ROWS).astype(BF16)
        for m in range(128 // cap):
            send[k * (128 // cap) + m] = picked[m * cap : (m + 1) * cap]

    pl.semaphore_wait(barrier, len(ep_peers) + n_tp - 1)

    own_rows = pl.ds(pl.multiple_of(x * cap, cap), cap)
    for g, pz, px in ep_peers:
        rcopy(ms_send_buf.at[pz], ms_in.at[g * NX + x], ms_s, ms_r, pz * NX + px, tp).start()
        rcopy(
            send.at[pz * NX + px], gathered.at[tp, g, own_rows], a2a_s, a2a_r.at[g], pz * NX + px, tp
        ).start()
    gathered[tp, 0, own_rows, :] = send[ep]
    ms_in[x] = ms_send_buf[z]
    for k, wtmp in ((3, wtmp_g), (4, wtmp_u)):
        loads[k].wait()

        def place(i, carry, wtmp=wtmp, at=(k - 3) * hpad):
            block = pl.ds(pl.multiple_of(i * 128, 128), 128)
            w2[block, at : at + hidden] = wtmp[block, :]
            return carry

        lax.fori_loop(0, width // 128, place, 0)
    loads[5].wait()

    def to_partner(share, g):
        piece = gathered.at[share, g]
        rcopy(piece, piece, pr_s, pr_r.at[g], ep, partner).start()

    def stage1(g):
        if g == 0:
            wait_in(gathered.at[tp, 0, pl.ds(0, group - cap)], a2a_s, a2a_r.at[0])
        else:
            wait_in(gathered.at[tp, g], a2a_s, a2a_r.at[g])
        piece = gathered.at[tp, g]
        rcopy(piece, piece, up_s, up_r.at[g], ep, tp_up).start()
        rcopy(piece, piece, dn_s, dn_r.at[g], ep, tp_dn).start()
        to_partner(tp, g)

    def stage2(g):
        below, above = gathered.at[tp_dn, g], gathered.at[tp_up, g]
        wait_in(below, up_s, up_r.at[g])
        if g % 2 == 0:
            rcopy(below, below, two_up_s, two_r.at[g], ep, tp_up).start()
        to_partner(tp_dn, g)
        wait_in(above, dn_s, dn_r.at[g])
        if g % 2 == 1:
            rcopy(above, above, two_dn_s, two_r.at[g], ep, tp_dn).start()
        to_partner(tp_up, g)

    def stage3(g):
        wait_in(gathered.at[tp_far, g], two_up_s, two_r.at[g])
        to_partner(tp_far, g)

    def stage4(g):
        wait_in(gathered.at[pl.ds(0, NY), g], pr_s, pr_r.at[g])

    def compute(q):
        at = slice(2 * q, 2 * q + 2)

        def part(k, lo):
            return gathered[k, at, :, lo : lo + cols].reshape(chunk, cols)

        xs = jnp.concatenate([part(k, 0) for k in range(n_tp)], axis=1)
        pre_g[...] = dot(xs, w2[:, :hpad])
        pre_u[...] = dot(xs, w2[:, hpad:])
        ys = jnp.concatenate([part(k, cols) for k in range(n_tp)], axis=1)
        back[...] = dot(ys, wd[...], OVER_COLS)
        if q == 0:
            wait_in(ms_in.at[pl.ds(0, n_ep - 1)], ms_s, ms_r)
        mine = iota((cap, 128), 1) == iota((cap, 128), 0) + x * cap
        spread = jnp.where(mine[None], ms_in[2 * q * NX : (2 * q + 2) * NX], 0.0)
        ms_col[pl.ds(q * chunk, chunk), :] = jnp.sum(spread, axis=2, keepdims=True).reshape(chunk, 1)

        def element(i, carry):
            block = pl.ds(pl.multiple_of(i * 32, 32), 32)
            out = pl.ds(pl.multiple_of(q * chunk + i * 32, 32), 32)
            a, u, b = pre_g[block, :], pre_u[block, :], back[block, :]
            sig = jax.nn.sigmoid(a)
            active = a * sig
            h = (active * u).astype(BF16)
            hid[block, :] = h
            mix_col[block, :] = jnp.sum(h.astype(F32) * b, axis=1, keepdims=True)
            scaled = ms_col[out, :] * b
            gu[out, :hpad] = (scaled * u * sig * (1.0 + a * (1.0 - sig))).astype(BF16)
            gu[out, hpad:] = (scaled * active).astype(BF16)
            return carry

        lax.fori_loop(0, chunk // 32, element, 0)
        eye = iota((group, group), 0) == iota((group, group), 1)
        for m in range(2):
            column = mix_col[m * group : (m + 1) * group, :]
            mix_row[2 * q + m] = jnp.sum(jnp.where(eye, column, 0.0), axis=0, keepdims=True)
        hid_t[:, q * chunk : (q + 1) * chunk] = hid[...].T

        def term(k, carry):
            w = w2[pl.ds(pl.multiple_of(k * cols, cols), cols), :]
            t = dot(gu[pl.ds(q * chunk, chunk), :], w, OVER_COLS)
            terms[lax.rem(k, 2), k // 2, at] = t.astype(BF16).reshape(2, group, cols)
            return carry

        lax.fori_loop(0, n_tp, term, 0)

    def rs_a(q):
        both_g = pl.ds(2 * q, 2)
        rcopy(terms.at[1 - core, :, both_g], pair_in.at[:, both_g], ra_s, ra_r.at[q], ep, partner).start()

    def add_into(ref, index, other):
        ref[index] = (ref[index].astype(F32) + other.astype(F32)).astype(BF16)

    yu, yd, yf = ring(y, 1, NY), ring(y, -1, NY), ring(y, 2, NY)

    def rs_bc(q):
        both_g = pl.ds(2 * q, 2)
        wait_in(pair_in.at[:, both_g], ra_s, ra_r.at[q])
        for k in (yf, yu, yd, y):
            for g in (2 * q, 2 * q + 1):
                add_into(terms, (core, k, g), pair_in[k, g])
        rcopy(terms.at[core, yf, 2 * q], near_a.at[q], rb_s, rb_r.at[q], ep, tp_up).start()
        rcopy(terms.at[core, yf, 2 * q + 1], near_b.at[q], rc_s, rc_r.at[q], ep, tp_dn).start()

    def rs_de(q):
        both_g = pl.ds(2 * q, 2)
        wait_in(near_a.at[q], rb_s, rb_r.at[q])
        add_into(terms, (core, yu, 2 * q), near_a[q])
        rcopy(terms.at[core, yu, both_g], far_p.at[both_g], rd_s, rd_r.at[q], ep, tp_up).start()
        wait_in(near_b.at[q], rc_s, rc_r.at[q])
        add_into(terms, (core, yd, 2 * q + 1), near_b[q])
        rcopy(terms.at[core, yd, both_g], far_m.at[both_g], re_s, re_r.at[q], ep, tp_dn).start()

    def rs_fg(q):
        both_g = pl.ds(2 * q, 2)
        wait_in(far_p.at[both_g], rd_s, rd_r.at[q])
        wait_in(far_m.at[both_g], re_s, re_r.at[q])
        for g in (2 * q, 2 * q + 1):
            summed = terms[core, y, g].astype(F32) + far_p[g].astype(F32) + far_m[g].astype(F32)
            total[g] = summed.astype(BF16)
            for dx in range(NX):
                if not (g or dx):
                    continue
                pz, px = ring(z, offsets[g], nz), ring(x, dx, NX)
                piece = total.at[g, pl.ds(pl.multiple_of(px * cap, cap), cap)]
                rcopy(piece, ret_in.at[ep], ret_s, ret_r, pz * NX + px, tp).start()
        if q == 0:
            ret_in[ep] = total[0, own_rows, :]

    def weights(k, carry):
        def all_rows(lo):
            return gathered[k, :, :, lo : lo + cols].reshape(slots, cols)

        at = pl.ds(pl.multiple_of(k * cols, cols), cols)
        both_grads = dot(all_rows(0), gu[...], OVER_ROWS)
        gate_grad_ref[at, :] = both_grads[:, :hidden].astype(BF16)
        up_grad_ref[at, :] = both_grads[:, hpad : hpad + hidden].astype(BF16)
        scaled = (ms_col[...] * all_rows(cols).astype(F32)).astype(BF16)
        down_grad_ref[:, at] = dot(hid_t[...], scaled)[:hidden].astype(BF16)
        return carry

    for s in range(nz + 3):
        if s < nz:
            stage1(s)
        if 0 <= s - 1 < nz:
            stage2(s - 1)
        if 0 <= s - 2 < nz:
            stage3(s - 2)
        if 0 <= s - 3 < nz:
            stage4(s - 3)
            if (s - 3) % 2:
                q = (s - 3) // 2
                compute(q)
                rs_a(q)
                if q >= 1:
                    rs_bc(q - 1)
                if q >= 2:
                    rs_de(q - 2)
                if q >= 3:
                    rs_fg(q - 3)

    mix_all[tp] = mix_row[...]
    for d in range(1, n_tp):
        rcopy(mix_row, mix_all.at[tp], mt_s, mt_r, ep, ring(tp, d, n_tp)).start()
    piece_k = n_tp // 4
    rs_bc(chunks - 1)
    rs_de(chunks - 2)
    lax.fori_loop(0, piece_k, weights, 0)
    rs_fg(chunks - 3)
    wait_in(mix_all.at[pl.ds(0, n_tp - 1)], mt_s, mt_r)
    mix_sum = mix_all[0]
    for k in range(1, n_tp):
        mix_sum = mix_sum + mix_all[k]
    mix_tot[...] = mix_sum
    mix_in[ep] = mix_tot[0]
    for g, dz in enumerate(offsets):
        for dx in range(NX):
            if g or dx:
                peer = ring(z, dz, nz) * NX + ring(x, dx, NX)
                rcopy(mix_tot.at[g], mix_in.at[ep], mx_s, mx_r, peer, tp).start()
    rs_de(chunks - 1)
    rs_fg(chunks - 2)
    lax.fori_loop(piece_k, 2 * piece_k, weights, 0)
    rs_fg(chunks - 1)

    wait_in(mix_in.at[pl.ds(0, n_ep - 1)], mx_s, mx_r)
    for e in range(n_ep):
        mix_mat[e : e + 1, :] = mix_in[e]
    rank0, rank1, mix0, mix1 = (small[:, k : k + 1] for k in range(4))
    r0, r1 = routes_ref[:, 0:1], routes_ref[:, 1:2]
    lane_f = (lanes - x * cap).astype(F32)
    lane_e = iota((rows, experts), 1)

    def own_grad(route, rank):
        chosen = jnp.where(route == lane_e, 1.0, 0.0)
        spread = lax.dot_general(
            chosen, mix_mat[...], (((1,), (0,)), ((), ())),
            precision=lax.Precision.HIGHEST, preferred_element_type=F32,
        )
        return jnp.sum(jnp.where(rank == lane_f, spread, 0.0), axis=1, keepdims=True)

    grad0, grad1 = own_grad(r0, rank0), own_grad(r1, rank1)
    mixing_ref[:, 0:1] = grad0
    mixing_ref[:, 1:2] = grad1
    pairwise = mix0 * mix1
    route_grad = jnp.where(r0 == lanes, pairwise * (grad0 - grad1), 0.0)
    route_grad = route_grad + jnp.where(r1 == lanes, pairwise * (grad1 - grad0), 0.0)
    rg_hi, rg_lo = halves(route_grad)
    scale = 1.0 / math.sqrt(rows * n_ep)

    def router_part(k, carry):
        at = pl.ds(pl.multiple_of(k * cols, cols), cols)
        t = tok[:, at]
        rparts[at, :] = (dot(t, rg_hi, OVER_ROWS) + dot(t, rg_lo, OVER_ROWS)) * scale
        return carry

    lax.fori_loop(0, n_tp, router_part, 0)
    share = width // (n_ep * n_tp)

    def share_rows(e):
        return pl.ds(pl.multiple_of((e * n_tp + tp) * share, share), share)

    for _, pz, px in ep_peers:
        peer = pz * NX + px
        rcopy(rparts.at[share_rows(peer)], rin.at[ep], rt_s, rt_r, peer, tp).start()
    rin[ep] = rparts[share_rows(ep), :]
    router_rows = router[pl.ds(pl.multiple_of(tp * cols, cols), cols), :]
    path = dot(rg_hi[:, :experts], router_rows, OVER_COLS)
    path = path + dot(rg_lo[:, :experts], router_rows, OVER_COLS)
    lax.fori_loop(2 * piece_k, n_tp, weights, 0)

    wait_in(ret_in.at[pl.ds(0, n_ep - 1)], ret_s, ret_r)
    token_part = dot(two_hot[...], ret_in[...].reshape(slots, cols))
    token_grad_ref[...] = (token_part + path).astype(BF16)
    wait_in(rin.at[pl.ds(0, n_ep - 1)], rt_s, rt_r)
    acc = rin[0]
    for e in range(1, n_ep):
        acc = acc + rin[e]
    router_grad_ref[...] = acc[:, :experts]

    wait_out(ms_in.at[pl.ds(0, n_ep - 1)], ms_s, ms_r)
    wait_out(send.at[pl.ds(0, n_ep - 1)], a2a_s, a2a_r.at[0])
    wait_out(gathered.at[0], up_s, up_r.at[0])
    wait_out(gathered.at[0], dn_s, dn_r.at[0])
    wait_out(gathered.at[0, pl.ds(0, nz // 2)], two_up_s, two_r.at[0])
    wait_out(gathered.at[0, pl.ds(0, nz // 2)], two_dn_s, two_r.at[0])
    wait_out(gathered.at[pl.ds(0, NY)], pr_s, pr_r.at[0])
    wait_out(pair_in, ra_s, ra_r.at[0])
    wait_out(near_a, rb_s, rb_r.at[0])
    wait_out(near_b, rc_s, rc_r.at[0])
    wait_out(far_p, rd_s, rd_r.at[0])
    wait_out(far_m, re_s, re_r.at[0])
    wait_out(mix_all.at[pl.ds(0, n_tp - 1)], mt_s, mt_r)
    wait_out(mix_in.at[pl.ds(0, n_ep - 1)], mx_s, mx_r)
    wait_out(rin.at[pl.ds(0, n_ep - 1)], rt_s, rt_r)
    wait_out(ret_in.at[pl.ds(0, n_ep - 1)], ret_s, ret_r)


def solution(mesh):
    n_ep, n_tp = mesh.shape["ep"], mesh.shape["tp"]

    def local(tokens, routes, router_matrix, cotangent, gate_proj, up_proj, down_proj):
        rows, width = tokens.shape
        experts = router_matrix.shape[1]
        hidden = gate_proj.shape[2]
        hpad = -(-hidden // 128) * 128
        cap = rows * 2 * 2 // experts
        slots = experts * cap
        cols = width // n_tp
        nz = n_ep // NX
        group = NX * cap
        chunk, chunks = 2 * group, nz // 2
        share = width // (n_ep * n_tp)
        dma = pltpu.SemaphoreType.DMA
        vmem = pltpu.VMEM
        any_ = pl.BlockSpec(memory_space=pl.ANY)
        whole = pl.BlockSpec(memory_space=pltpu.VMEM)
        scratch = [
            vmem((rows, width), BF16), vmem((rows, cols), BF16), vmem((width, experts), BF16),
            vmem((width, hidden), BF16), vmem((width, hidden), BF16),
            vmem((width, 2 * hpad), BF16), vmem((hpad, width), BF16),
            vmem((n_ep, cap, 2 * cols), BF16), vmem((slots // 128, 1, 128), F32),
            vmem((rows, slots), BF16), vmem((rows, 128), F32),
            vmem((n_tp, nz, group, 2 * cols), BF16), vmem((n_ep, 1, 128), F32),
            vmem((chunk, hpad), F32), vmem((chunk, hpad), F32), vmem((chunk, hpad), F32),
            vmem((chunk, hpad), BF16), vmem((hpad, slots), BF16), vmem((slots, 2 * hpad), BF16),
            vmem((slots, 1), F32), vmem((chunk, 1), F32),
            vmem((2, NY, nz, group, cols), BF16), vmem((NY, nz, group, cols), BF16),
            vmem((chunks, group, cols), BF16), vmem((chunks, group, cols), BF16),
            vmem((nz, group, cols), BF16), vmem((nz, group, cols), BF16),
            vmem((nz, group, cols), BF16), vmem((n_ep, cap, cols), BF16),
            vmem((nz, 1, 128), F32), vmem((n_tp, nz, 1, 128), F32), vmem((nz, 1, 128), F32),
            vmem((n_ep, 1, 128), F32), vmem((n_ep, 128), F32),
            vmem((width, 128), F32), vmem((n_ep, share, 128), F32),
            dma((6,)),
            dma, dma, dma, dma((nz,)), dma, dma((nz,)), dma, dma((nz,)), dma, dma, dma((nz,)),
            dma, dma((nz,)),
            dma, dma((chunks,)), dma, dma((chunks,)), dma, dma((chunks,)), dma, dma((chunks,)),
            dma, dma((chunks,)),
            dma, dma, dma, dma, dma, dma, dma, dma,
        ]
        shape = jax.ShapeDtypeStruct
        token_grad, mixing, router_grad, gate_grad, up_grad, down_grad = pl.pallas_call(
            lambda *refs: kernel(n_ep, n_tp, *refs),
            out_shape=(
                shape((rows, cols), BF16), shape((rows, 2), F32), shape((share, experts), F32),
                shape((width, hidden), BF16), shape((width, hidden), BF16),
                shape((hidden, width), BF16),
            ),
            in_specs=[any_, whole, any_, any_, any_, any_, any_],
            out_specs=(whole,) * 6,
            scratch_shapes=scratch,
            compiler_params=pltpu.CompilerParams(
                collective_id=0, has_side_effects=True, vmem_limit_bytes=66 * 1024 * 1024 - 2**21
            ),
            name="moe_backward",
        )(tokens, routes, router_matrix, cotangent, gate_proj, up_proj, down_proj)
        return token_grad, mixing, router_grad, gate_grad[None], up_grad[None], down_grad[None]

    return jax.shard_map(
        local,
        mesh=mesh,
        in_specs=(
            P("ep", None), P("ep", None), P(), P("ep", "tp"),
            P("ep", None, "tp"), P("ep", None, "tp"), P("ep", "tp", None),
        ),
        out_specs=(
            P("ep", "tp"), P("ep", None), P(("ep", "tp"), None),
            P("ep", None, "tp"), P("ep", None, "tp"), P("ep", "tp", None),
        ),
        check_vma=False,
    )
```

time: 236 us -> 128 us (0.54)
  Pallas kernels: 0 us -> 105 us
  waiting for transfers between devices: 73 us -> 0 us
  blocking collectives: 46.4 us -> 0 us
  matrix products: 34.1 us -> 0 us
  starting transfers between devices: 24.6 us -> 0 us
  between operations: 14.5 us -> 0.65 us
  local copies, waits for them, and re-layouts: 35.2 us -> 21.8 us
  other arithmetic: 7.21 us -> 0 us
    pallas_call x0 -> x1, Pallas kernels: none -> 105 us  [local(): pl.pallas_call(lambda *refs: kernel(n_ep, n_tp, *refs), out_shape=(shape(...]
    all_gather x1 -> x0, waiting for transfers between devices: 51.2 us -> none  [side_by_side_2(): whole, at, done = (lax.all_gather(both, axis, axis=dim, tiled=True), 0, [])]
    all_to_all x1 -> x0, blocking collectives: 46.4 us -> none  [side_by_side(): lax.all_to_all(both, axis, split_axis=split_dim, concat_axis=concat_dim,...]
    dot_general x11 -> x0, matrix products: 34.1 us -> none  [the longest x1 5.84 us: local(): lax.dot_general(token_rows, gate_back, over_rows, preferred_element_type=...]
    all_to_all x4 -> x0, starting transfers between devices: 24.3 us -> none  [the longest x1 10 us: local(): lax.all_to_all(mix_total, 'ep', split_axis=0, concat_axis=0, tiled=True)]
    all_to_all x4 -> x0, waiting for transfers between devices: 21.7 us -> none  [the longest x1 8.13 us: local(): lax.all_to_all(mix_total, 'ep', split_axis=0, concat_axis=0, tiled=True)]
    gather x5 -> x0, local copies, waits for them, and re-layouts: 18.9 us -> none  [the longest x1 6.8 us: local(): mixing.reshape(-1)[entry_src]]
    unnamed x33 -> x18, local copies, waits for them, and re-layouts: 5.24 us -> 21.8 us
  transfers between devices with their start and end apart: 6 -> 0, of which waited for: 5 -> 0; matrix products, arithmetic and copies ran while one was open for 11% -> 0% of each run, Pallas kernels for 0% -> 0%
where the time goes in v1:
time: 128 us; the launch traced here: 127 us
  Pallas kernels  105 us (82%)
  local copies, waits for them, and re-layouts  21.8 us (17%)
    pallas_call x1, Pallas kernels, local(): pl.pallas_call(lambda *refs: kernel(n_ep, n_tp, *refs), out_shape=(shape(...  105 us
    unnamed x18, local copies, waits for them, and re-layouts  21.8 us

profile of v1, /device:TPU:8, one launch (start us, length us, event | category | flops | bytes accessed | tf_op | source)
XLA Modules:
  0.0 127.5 jit_solution(13027889553712006017)
XLA Ops:
  0.6 1.5 %copy.13.refs_1_ = s32[256,2]{1,0:T(8,128)} copy(s32[256,2]{0,1:T(2,128)} %param.8) | data formatting | bytes 4096 | tf_op args[1]
  2.1 1.9 %copy.14.refs_2_ = bf16[2048,32]{1,0:T(8,128)(2,1)} copy(bf16[2048,32]{0,1:T(8,128)(2,1)} %param.9) | data formatting | bytes 262144 | tf_op args[2]
  4.0 0.0 copy-start.1
  4.0 3.9 %copy.15.refs_4_ = bf16[1,2048,448]{2,1,0:T(8,128)(2,1)} copy(bf16[1,2048,448]{1,2,0:T(8,128)(2,1)} %param.11) | data formatting | bytes 3670016 | tf_op args[4]
  8.0 0.0 copy-done.1
  8.0 2.4 %copy.16.refs_5_ = bf16[1,2048,448]{2,1,0:T(8,128)(2,1)} copy(bf16[1,2048,448]{1,2,0:T(8,128)(2,1)S(1)} %copy-done.1) | data formatting | bytes 3670016 | tf_op args[5]
  10.4 105.1 %moe_backward.1 = (bf16[256,256]{1,0:T(8,128)(2,1)}, f32[256,2]{1,0:T(8,128)}, f32[8,32]{1,0:T(8,128)}, bf16[2048,448]{1,0:T(8,128)(2,1)}, bf16[2048,448]{1,0:T(8,128)(2,1)}, /*index=5*/bf16[448,2048]{1,0:T(8,128)(2,1)}) custom-call(bf16[256,2048]{1,0:T(8,128)(2,1)} %refs_0_.1, s32[256,2]{1,0:T(8,128)} %copy.13.refs_1_, bf16[2048,32]{1,0:T(8,128)(2,1)} %copy.14.refs_2_, ...), custom_call_target="tpu_custom_call" | custom-call | tf_op jit(solution)/shard_map/moe_backward/pallas_call | solution.py:466
  115.4 1.6 %copy.17 = f32[256,2]{0,1:T(2,128)} copy(f32[256,2]{1,0:T(8,128)} %get-tuple-element.19) | data formatting | bytes 4096
  117.0 0.0 copy-start
  117.0 4.0 %copy.18 = bf16[1,2048,448]{1,2,0:T(8,128)(2,1)} copy(bf16[1,2048,448]{2,1,0:T(8,128)(2,1)} %bitcast.4) | data formatting | bytes 3670016
  121.0 0.0 copy-done
  121.0 0.0 copy-start.2
  121.0 0.0 copy-start.3
  121.0 2.3 %copy.19 = bf16[1,2048,448]{1,2,0:T(8,128)(2,1)} copy(bf16[1,2048,448]{2,1,0:T(8,128)(2,1)S(1)} %bitcast.3) | data formatting | bytes 3670016
  123.3 0.0 copy-done.2
  123.3 0.7 copy.23
  124.0 0.0 copy-done.3
  124.0 0.6 copy.24
  124.6 2.9 %copy.25 = bf16[1,448,2048]{2,1,0:T(8,128)(2,1)} copy(bf16[1,448,2048]{2,1,0:T(8,128)(2,1)} %bitcast.5) | data formatting | bytes 3670016
Async XLA Ops:
  4.0 3.9 %copy-start.1 = (bf16[1,2048,448]{1,2,0:T(8,128)(2,1)S(1)}, bf16[1,2048,448]{1,2,0:T(8,128)(2,1)}, u32[]{:S(2)}) copy-start(bf16[1,2048,448]{1,2,0:T(8,128)(2,1)} %param.12) | copy-start | bytes 5505028
  117.0 4.0 %copy-start = (bf16[2048,448]{1,0:T(8,128)(2,1)S(1)}, bf16[2048,448]{1,0:T(8,128)(2,1)}, u32[]{:S(2)}) copy-start(bf16[2048,448]{1,0:T(8,128)(2,1)} %get-tuple-element.16) | copy-start | bytes 5505028
  121.0 2.3 %copy-start.2 = (bf16[256,256]{1,0:T(8,128)(2,1)S(1)}, bf16[256,256]{1,0:T(8,128)(2,1)}, u32[]{:S(2)}) copy-start(bf16[256,256]{1,0:T(8,128)(2,1)} %get-tuple-element.30) | copy-start | bytes 393220
  121.0 3.0 %copy-start.3 = (f32[8,32]{1,0:T(8,128)S(1)}, f32[8,32]{1,0:T(8,128)}, u32[]{:S(2)}) copy-start(f32[8,32]{1,0:T(8,128)} %get-tuple-element.32) | copy-start | bytes 3076

commit v2 on v1

v2 whole, which is shorter than its diff:
```python
import math

import jax
import jax.numpy as jnp
from jax import lax
from jax.experimental import pallas as pl
from jax.experimental.pallas import tpu as pltpu
from jax.sharding import PartitionSpec as P

MESH = pl.DeviceIdType.MESH
BF16 = jnp.bfloat16
F32 = jnp.float32

NX, NY = 4, 4
OFFSETS = (0, 1, -2, 3, -3, 4, -1, 2)
VMEM_LIMIT = 47 * 2**20
OVER_ROWS = (((0,), (0,)), ((), ()))
OVER_COLS = (((1,), (1,)), ((), ()))


def dot(a, b, dims=None):
    if dims is None:
        return jnp.dot(a, b, preferred_element_type=F32)
    return lax.dot_general(a, b, dims, preferred_element_type=F32)


def iota(shape, dim):
    return lax.broadcasted_iota(jnp.int32, shape, dim)


def phase(step):
    def named(k):
        with jax.named_scope(step.__name__ + str(k)):
            return step(k)

    return named


def halves(value):
    high = value.astype(BF16)
    return high, (value - high.astype(F32)).astype(BF16)


def kernel(
    n_ep, n_tp, hidden,
    tokens_h, routes_ref, router_h, cot_h, gate_h, up_h, down_h,
    token_grad_ref, mixing_ref, router_grad_ref, gate_grad_ref, up_grad_ref, down_grad_ref,
    tok, cot, router, w2, wd, w2_t, wd_t,
    send, ms_send_buf, two_hot, small, gathered, ms_in,
    pre, back, hid, hid_t, gu, gu_t, ms_col, mix_col,
    terms, pair_in, near_a, near_b, far_p, far_m, total, ret_in,
    mix_row, mix_all, mix_tot, mix_in, mix_mat, rparts, rin,
    lsem,
    ms_s, ms_r, a2a_s, a2a_r, up_s, up_r, dn_s, dn_r, two_up_s, two_dn_s, two_r, pr_s, pr_r,
    ra_s, ra_r, rb_s, rb_r, rc_s, rc_r, rd_s, rd_r, re_s, re_r,
    mt_s, mt_r, mx_s, mx_r, rt_s, rt_r, ret_s, ret_r,
):
    nz = n_ep // NX
    rows, width = tok.shape
    experts = router.shape[0]
    cap = rows * 2 * 2 // experts
    cols = width // n_tp
    hpad = wd.shape[0]
    slots = experts * cap
    group = NX * cap
    chunk = 2 * group
    chunks = nz // 2
    ep, tp = lax.axis_index("ep"), lax.axis_index("tp")
    z, x = ep // NX, lax.rem(ep, NX)
    y, core = tp // 2, lax.rem(tp, 2)
    offsets = OFFSETS
    home = offsets.index(0)

    def ring(value, step, size):
        return lax.rem(value + (step + size), size)

    def tp_of(step):
        return ring(y, step, NY) * 2 + core

    tp_up, tp_dn, tp_far = tp_of(1), tp_of(-1), tp_of(2)
    partner = y * 2 + (1 - core)

    def rcopy(src, dst, s, r, e, t):
        return pltpu.make_async_remote_copy(
            src_ref=src, dst_ref=dst, send_sem=s, recv_sem=r, device_id=(e, t), device_id_type=MESH
        )

    def wait_in(ref, s, r):
        rcopy(ref, ref, s, r, ep, partner).wait_recv()

    def wait_out(ref, s, r):
        rcopy(ref, ref, s, r, ep, partner).wait_send()

    ep_peers = []
    for g, dz in enumerate(offsets):
        for dx in range(NX):
            if dz or dx:
                ep_peers.append((g, ring(z, -dz, nz), ring(x, dx, NX)))

    barrier = pltpu.get_barrier_semaphore()
    for _, pz, px in ep_peers:
        pl.semaphore_signal(barrier, inc=1, device_id=(pz * NX + px, tp), device_id_type=MESH)
    for d in range(1, n_tp):
        pl.semaphore_signal(barrier, inc=1, device_id=(ep, ring(tp, d, n_tp)), device_id_type=MESH)
    loads = [
        pltpu.make_async_copy(a, b, lsem.at[k])
        for k, (a, b) in enumerate(
            (
                (tokens_h, tok), (router_h, router), (cot_h, cot),
                (gate_h.at[0], w2.at[pl.ds(0, hidden)]),
                (up_h.at[0], w2.at[pl.ds(hpad, hidden)]),
                (down_h.at[0], wd.at[pl.ds(0, hidden)]),
            )
        )
    ]
    for load in loads:
        load.start()
    gap = jnp.zeros((hpad - hidden, width), BF16)
    w2[hidden:hpad, :] = gap
    w2[hpad + hidden :, :] = gap
    wd[hidden:, :] = gap
    with jax.named_scope("load"):
        loads[0].wait()
        loads[1].wait()

    lanes = iota((rows, 128), 1)
    diagonal = iota((rows, rows), 0) == iota((rows, rows), 1)

    def column(row):
        return jnp.sum(jnp.where(diagonal, row, 0.0), axis=1, keepdims=True)

    r0, r1 = (column(routes_ref[k : k + 1, :].astype(F32)) for k in range(2))
    lanes_f = lanes.astype(F32)
    oh0, oh1 = r0 == lanes_f, r1 == lanes_f
    both = jnp.where(oh0 | oh1, 1.0, 0.0).astype(BF16)
    before = jnp.where(iota((rows, rows), 0) > iota((rows, rows), 1), 1.0, 0.0).astype(BF16)
    earlier = dot(before, both)
    rank0 = jnp.sum(jnp.where(oh0, earlier, 0.0), axis=1, keepdims=True)
    rank1 = jnp.sum(jnp.where(oh1, earlier, 0.0), axis=1, keepdims=True)
    logits = dot(tok[...], router[...], OVER_COLS)
    lane_e = iota((rows, experts), 1).astype(F32)
    chosen0 = jnp.sum(jnp.where(r0 == lane_e, logits, 0.0), axis=1, keepdims=True)
    chosen1 = jnp.sum(jnp.where(r1 == lane_e, logits, 0.0), axis=1, keepdims=True)
    mix0 = jax.nn.sigmoid(chosen0 - chosen1)
    mix1 = jax.nn.sigmoid(chosen1 - chosen0)
    small[:, 0:1] = rank0
    small[:, 1:2] = rank1
    small[:, 2:3] = mix0
    small[:, 3:4] = mix1
    small[:, 4:5] = r0
    small[:, 5:6] = r1
    place0 = r0 * cap + rank0
    place1 = r1 * cap + rank1
    mb0 = mix0.astype(BF16).astype(F32)
    mb1 = mix1.astype(BF16).astype(F32)
    loads[2].wait()
    source = jnp.concatenate(
        [tok[:, pl.ds(pl.multiple_of(tp * cols, cols), cols)], cot[...]], axis=1
    )
    for k in range(slots // 128):
        at = (iota((rows, 128), 1) + k * 128).astype(F32)
        hit0, hit1 = place0 == at, place1 == at
        chosen = jnp.where(hit0 | hit1, 1.0, 0.0).astype(BF16)
        two_hot[:, k * 128 : (k + 1) * 128] = chosen
        ms_send_buf[k] = jnp.sum(
            jnp.where(hit0, mb0, 0.0) + jnp.where(hit1, mb1, 0.0), axis=0, keepdims=True
        )
        picked = dot(chosen, source, OVER_ROWS).astype(BF16)
        for m in range(128 // cap):
            send[k * (128 // cap) + m] = picked[m * cap : (m + 1) * cap]

    with jax.named_scope("barrier"):
        pl.semaphore_wait(barrier, len(ep_peers) + n_tp - 1)

    own_rows = pl.ds(pl.multiple_of(x * cap, cap), cap)
    for g, pz, px in ep_peers:
        peer, land = pz * NX + px, gathered.at[tp, g, own_rows]
        rcopy(ms_send_buf.at[pz], ms_in.at[g * NX + x], ms_s, ms_r, peer, tp).start()
        rcopy(send.at[peer], land, a2a_s, a2a_r.at[g], peer, tp).start()
    gathered[tp, home, own_rows, :] = send[ep]
    ms_in[home * NX + x] = ms_send_buf[z]
    with jax.named_scope("weights_in"):
        for load in loads[3:]:
            load.wait()

        def flip(k, carry):
            at = pl.ds(pl.multiple_of(k * cols, cols), cols)
            w2_t[at, :] = w2[:, at].T
            wd_t[at, :] = wd[:, at].T
            return carry

        lax.fori_loop(0, n_tp, flip, 0)

    def to_partner(share, g):
        piece = gathered.at[share, g]
        rcopy(piece, piece, pr_s, pr_r.at[g], ep, partner).start()

    @phase
    def stage1(g):
        if g == home:
            wait_in(gathered.at[tp, g, pl.ds(0, group - cap)], a2a_s, a2a_r.at[g])
        else:
            wait_in(gathered.at[tp, g], a2a_s, a2a_r.at[g])
        piece = gathered.at[tp, g]
        rcopy(piece, piece, up_s, up_r.at[g], ep, tp_up).start()
        rcopy(piece, piece, dn_s, dn_r.at[g], ep, tp_dn).start()
        to_partner(tp, g)

    @phase
    def stage2(g):
        below, above = gathered.at[tp_dn, g], gathered.at[tp_up, g]
        wait_in(below, up_s, up_r.at[g])
        if g % 2 == 0:
            rcopy(below, below, two_up_s, two_r.at[g], ep, tp_up).start()
        to_partner(tp_dn, g)
        wait_in(above, dn_s, dn_r.at[g])
        if g % 2 == 1:
            rcopy(above, above, two_dn_s, two_r.at[g], ep, tp_dn).start()
        to_partner(tp_up, g)

    @phase
    def stage3(g):
        wait_in(gathered.at[tp_far, g], two_up_s, two_r.at[g])
        to_partner(tp_far, g)

    @phase
    def stage4(g):
        wait_in(gathered.at[pl.ds(0, NY), g], pr_s, pr_r.at[g])

    def rows_of(q, lo):
        at = slice(2 * q, 2 * q + 2)
        return jnp.concatenate(
            [gathered[k, at, :, lo : lo + cols].reshape(chunk, cols) for k in range(n_tp)], axis=1
        )

    @phase
    def forward(q):
        pre[...] = dot(rows_of(q, 0), w2_t[...])

    @phase
    def backward(q):
        back[...] = dot(rows_of(q, cols), wd_t[...])
        if q == 0:
            wait_in(ms_in.at[pl.ds(0, n_ep - 1)], ms_s, ms_r)
        mine = iota((cap, 128), 1) == iota((cap, 128), 0) + x * cap
        spread = jnp.where(mine[None], ms_in[2 * q * NX : (2 * q + 2) * NX], 0.0)
        ms_col[pl.ds(q * chunk, chunk), :] = jnp.sum(spread, axis=2, keepdims=True).reshape(chunk, 1)

    @phase
    def element(q):
        def block_of(i, carry):
            block = pl.ds(pl.multiple_of(i * 32, 32), 32)
            out = pl.ds(pl.multiple_of(q * chunk + i * 32, 32), 32)
            a, u, b = pre[block, :hpad], pre[block, hpad:], back[block, :]
            sig = jax.nn.sigmoid(a)
            active = a * sig
            h = (active * u).astype(BF16)
            hid[block, :] = h
            mix_col[block, :] = jnp.sum(h.astype(F32) * b, axis=1, keepdims=True)
            scaled = ms_col[out, :] * b
            gu[out, :hpad] = (scaled * u * sig * (1.0 + a * (1.0 - sig))).astype(BF16)
            gu[out, hpad:] = (scaled * active).astype(BF16)
            return carry

        lax.fori_loop(0, chunk // 32, block_of, 0)

    @phase
    def term(q):
        def term_of(k, carry):
            w = w2[:, pl.ds(pl.multiple_of(k * 4 * cols, 4 * cols), 4 * cols)]
            t = dot(gu[pl.ds(q * chunk, chunk), :], w).astype(BF16)
            for m in range(4):
                piece = t[:, m * cols : (m + 1) * cols].reshape(2, group, cols)
                terms[m % 2, 2 * k + m // 2, 2 * q : 2 * q + 2] = piece
            return carry

        lax.fori_loop(0, n_tp // 4, term_of, 0)

    @phase
    def turn(q):
        eye = iota((group, group), 0) == iota((group, group), 1)
        for m in range(2):
            column = mix_col[m * group : (m + 1) * group, :]
            mix_row[2 * q + m] = jnp.sum(jnp.where(eye, column, 0.0), axis=0, keepdims=True)
        hid_t[:, q * chunk : (q + 1) * chunk] = hid[...].T
        gu_t[:, q * chunk : (q + 1) * chunk] = gu[q * chunk : (q + 1) * chunk, :].T

    @phase
    def rs_a(q):
        both_g = pl.ds(2 * q, 2)
        rcopy(terms.at[1 - core, :, both_g], pair_in.at[:, both_g], ra_s, ra_r.at[q], ep, partner).start()

    def add_into(ref, index, other):
        ref[index] = (ref[index].astype(F32) + other.astype(F32)).astype(BF16)

    yu, yd, yf = ring(y, 1, NY), ring(y, -1, NY), ring(y, 2, NY)

    @phase
    def rs_bc(q):
        both_g = pl.ds(2 * q, 2)
        wait_in(pair_in.at[:, both_g], ra_s, ra_r.at[q])
        for k in (yf, yu, yd, y):
            for g in (2 * q, 2 * q + 1):
                add_into(terms, (core, k, g), pair_in[k, g])
        rcopy(terms.at[core, yf, 2 * q], near_a.at[q], rb_s, rb_r.at[q], ep, tp_up).start()
        rcopy(terms.at[core, yf, 2 * q + 1], near_b.at[q], rc_s, rc_r.at[q], ep, tp_dn).start()

    @phase
    def rs_de(q):
        both_g = pl.ds(2 * q, 2)
        wait_in(near_a.at[q], rb_s, rb_r.at[q])
        add_into(terms, (core, yu, 2 * q), near_a[q])
        rcopy(terms.at[core, yu, both_g], far_p.at[both_g], rd_s, rd_r.at[q], ep, tp_up).start()
        wait_in(near_b.at[q], rc_s, rc_r.at[q])
        add_into(terms, (core, yd, 2 * q + 1), near_b[q])
        rcopy(terms.at[core, yd, both_g], far_m.at[both_g], re_s, re_r.at[q], ep, tp_dn).start()

    @phase
    def rs_fg(q):
        both_g = pl.ds(2 * q, 2)
        wait_in(far_p.at[both_g], rd_s, rd_r.at[q])
        wait_in(far_m.at[both_g], re_s, re_r.at[q])
        for g in (2 * q, 2 * q + 1):
            summed = terms[core, y, g].astype(F32) + far_p[g].astype(F32) + far_m[g].astype(F32)
            total[g] = summed.astype(BF16)
            for dx in range(NX):
                if g == home and dx == 0:
                    continue
                pz, px = ring(z, offsets[g], nz), ring(x, dx, NX)
                piece = total.at[g, pl.ds(pl.multiple_of(px * cap, cap), cap)]
                rcopy(piece, ret_in.at[ep], ret_s, ret_r, pz * NX + px, tp).start()
        if q == home // 2:
            ret_in[ep] = total[home, own_rows, :]

    def weights(k, carry):
        def all_rows(lo):
            return gathered[k, :, :, lo : lo + cols].reshape(slots, cols)

        at = pl.ds(pl.multiple_of(k * cols, cols), cols)
        both_grads = dot(gu_t[...], all_rows(0)).astype(BF16)
        gate_grad_ref[:, at] = both_grads[:hidden]
        up_grad_ref[:, at] = both_grads[hpad : hpad + hidden]
        scaled = (ms_col[...] * all_rows(cols).astype(F32)).astype(BF16)
        down_grad_ref[:, at] = dot(hid_t[...], scaled)[:hidden].astype(BF16)
        return carry

    def poll(k):
        if k < nz:
            stage2(k)
        if k + 2 < nz:
            stage1(k + 2)
        if k:
            stage3(k - 1)

    def ready(q):
        stage4(2 * q)
        stage4(2 * q + 1)

    def grads(lo, hi):
        with jax.named_scope("grads" + str(lo)):
            lax.fori_loop(lo, hi, weights, 0)

    def mix_out(q):
        both_g = pl.ds(2 * q, 2)
        mix_all[tp, both_g] = mix_row[both_g]
        for d in range(1, n_tp):
            peer = ring(tp, d, n_tp)
            rcopy(mix_row.at[both_g], mix_all.at[tp, both_g], mt_s, mt_r.at[q], ep, peer).start()

    @phase
    def mix_home(q):
        both_g = pl.ds(2 * q, 2)
        wait_in(mix_all.at[pl.ds(0, n_tp - 1), both_g], mt_s, mt_r.at[q])
        mix_sum = mix_all[0, both_g]
        for k in range(1, n_tp):
            mix_sum = mix_sum + mix_all[k, both_g]
        mix_tot[both_g] = mix_sum
        for g in (2 * q, 2 * q + 1):
            for dx in range(NX):
                if g == home and dx == 0:
                    mix_in[ep] = mix_tot[home]
                else:
                    peer = ring(z, offsets[g], nz) * NX + ring(x, dx, NX)
                    rcopy(mix_tot.at[g], mix_in.at[ep], mx_s, mx_r, peer, tp).start()

    stage1(0)
    stage1(1)
    for k in range(3):
        poll(k)
    last = chunks - 1
    for q in range(last):
        ready(q)
        forward(q)
        poll(2 * q + 3)
        if q >= 1:
            rs_bc(q - 1)
        backward(q)
        element(q)
        poll(2 * q + 4)
        term(q)
        rs_a(q)
        if q >= 1:
            rs_de(q - 1)
        if q >= 2:
            rs_fg(q - 2)
        turn(q)
        mix_out(q)
        if q >= 1:
            mix_home(q - 1)

    ready(last)
    forward(last)
    rs_bc(last - 1)
    backward(last)
    element(last)
    turn(last)
    mix_out(last)
    term(last)
    rs_a(last)
    rs_de(last - 1)
    mix_home(last - 1)
    mix_home(last)
    rs_fg(last - 2)
    rs_bc(last)
    grads(0, 2)
    rs_fg(last - 1)
    grads(2, 3)
    rs_de(last)

    with jax.named_scope("mix_wait"):
        wait_in(mix_in.at[pl.ds(0, n_ep - 1)], mx_s, mx_r)
    for e in range(n_ep):
        mix_mat[e : e + 1, :] = mix_in[e]
    rank0, rank1, mix0, mix1, r0, r1 = (small[:, k : k + 1] for k in range(6))
    lane_f = (lanes - x * cap).astype(F32)

    def own_grad(route, rank):
        chosen = jnp.where(route == lane_e, 1.0, 0.0)
        spread = lax.dot_general(
            chosen, mix_mat[...], (((1,), (0,)), ((), ())),
            precision=lax.Precision.HIGHEST, preferred_element_type=F32,
        )
        return jnp.sum(jnp.where(rank == lane_f, spread, 0.0), axis=1, keepdims=True)

    grad0, grad1 = own_grad(r0, rank0), own_grad(r1, rank1)
    mixing_ref[0:1, :] = jnp.sum(jnp.where(diagonal, grad0, 0.0), axis=0, keepdims=True)
    mixing_ref[1:2, :] = jnp.sum(jnp.where(diagonal, grad1, 0.0), axis=0, keepdims=True)
    pairwise = mix0 * mix1
    route_grad = jnp.where(r0 == lanes_f, pairwise * (grad0 - grad1), 0.0)
    route_grad = route_grad + jnp.where(r1 == lanes_f, pairwise * (grad1 - grad0), 0.0)
    rg_hi, rg_lo = halves(route_grad)
    scale = 1.0 / math.sqrt(rows * n_ep)
    share = width // (n_ep * n_tp)
    per = cols // share
    turned_hi, turned_lo = rg_hi.T, rg_lo.T
    with jax.named_scope("router_part"):
        for k in range(n_tp):
            t = tok[:, k * cols : (k + 1) * cols]
            part = ((dot(turned_hi, t) + dot(turned_lo, t)) * scale).T.astype(BF16)
            rparts[k * per : (k + 1) * per] = part.reshape(per, share, 128)
    for _, pz, px in ep_peers:
        peer = pz * NX + px
        rcopy(rparts.at[peer * n_tp + tp], rin.at[ep], rt_s, rt_r, peer, tp).start()
    rin[ep] = rparts[ep * n_tp + tp]
    router_cols = router[:, pl.ds(pl.multiple_of(tp * cols, cols), cols)]
    path = dot(rg_hi[:, :experts], router_cols) + dot(rg_lo[:, :experts], router_cols)
    grads(3, 5)
    rs_fg(last)
    grads(5, n_tp)

    with jax.named_scope("ret_wait"):
        wait_in(ret_in.at[pl.ds(0, n_ep - 1)], ret_s, ret_r)
    token_part = dot(two_hot[...], ret_in[...].reshape(slots, cols))
    token_grad_ref[...] = (token_part + path).astype(BF16)
    with jax.named_scope("router_wait"):
        wait_in(rin.at[pl.ds(0, n_ep - 1)], rt_s, rt_r)
    acc = rin[0].astype(F32)
    for e in range(1, n_ep):
        acc = acc + rin[e].astype(F32)
    router_grad_ref[...] = acc[:, :experts]

    wait_out(ms_in.at[pl.ds(0, n_ep - 1)], ms_s, ms_r)
    wait_out(send.at[pl.ds(0, n_ep - 1)], a2a_s, a2a_r.at[0])
    wait_out(gathered.at[0], up_s, up_r.at[0])
    wait_out(gathered.at[0], dn_s, dn_r.at[0])
    wait_out(gathered.at[0, pl.ds(0, nz // 2)], two_up_s, two_r.at[0])
    wait_out(gathered.at[0, pl.ds(0, nz // 2)], two_dn_s, two_r.at[0])
    wait_out(gathered.at[pl.ds(0, NY)], pr_s, pr_r.at[0])
    wait_out(pair_in, ra_s, ra_r.at[0])
    wait_out(near_a, rb_s, rb_r.at[0])
    wait_out(near_b, rc_s, rc_r.at[0])
    wait_out(far_p, rd_s, rd_r.at[0])
    wait_out(far_m, re_s, re_r.at[0])
    wait_out(mix_all.at[pl.ds(0, n_tp - 1)], mt_s, mt_r)
    wait_out(mix_in.at[pl.ds(0, n_ep - 1)], mx_s, mx_r)
    wait_out(rin.at[pl.ds(0, n_ep - 1)], rt_s, rt_r)
    wait_out(ret_in.at[pl.ds(0, n_ep - 1)], ret_s, ret_r)


def hand_over(*refs):
    count = len(refs) // 2
    copies = [
        pltpu.make_async_copy(refs[k], refs[count + k], refs[-1].at[k]) for k in range(count)
    ]
    for copy in copies:
        copy.start()
    for copy in copies:
        copy.wait()


def solution(mesh):
    n_ep, n_tp = mesh.shape["ep"], mesh.shape["tp"]

    def local(tokens, routes, router_matrix, cotangent, gate_proj, up_proj, down_proj):
        rows, width = tokens.shape
        experts = router_matrix.shape[1]
        hidden = gate_proj.shape[2]
        hpad = -(-hidden // 128) * 128
        cap = rows * 2 * 2 // experts
        slots = experts * cap
        cols = width // n_tp
        nz = n_ep // NX
        group = NX * cap
        chunk, chunks = 2 * group, nz // 2
        share = width // (n_ep * n_tp)
        dma = pltpu.SemaphoreType.DMA
        vmem = pltpu.VMEM
        any_ = pl.BlockSpec(memory_space=pltpu.HBM)
        whole = pl.BlockSpec(memory_space=pltpu.VMEM)
        scratch = [
            vmem((rows, width), BF16), vmem((rows, cols), BF16), vmem((experts, width), BF16),
            vmem((2 * hpad, width), BF16), vmem((hpad, width), BF16),
            vmem((width, 2 * hpad), BF16), vmem((width, hpad), BF16),
            vmem((n_ep, cap, 2 * cols), BF16), vmem((slots // 128, 1, 128), F32),
            vmem((rows, slots), BF16), vmem((rows, 128), F32),
            vmem((n_tp, nz, group, 2 * cols), BF16), vmem((n_ep, 1, 128), F32),
            vmem((chunk, 2 * hpad), F32), vmem((chunk, hpad), F32),
            vmem((chunk, hpad), BF16), vmem((hpad, slots), BF16), vmem((slots, 2 * hpad), BF16),
            vmem((2 * hpad, slots), BF16),
            vmem((slots, 1), F32), vmem((chunk, 1), F32),
            vmem((2, NY, nz, group, cols), BF16), vmem((NY, nz, group, cols), BF16),
            vmem((chunks, group, cols), BF16), vmem((chunks, group, cols), BF16),
            vmem((nz, group, cols), BF16), vmem((nz, group, cols), BF16),
            vmem((nz, group, cols), BF16), vmem((n_ep, cap, cols), BF16),
            vmem((nz, 1, 128), F32), vmem((n_tp, nz, 1, 128), F32), vmem((nz, 1, 128), F32),
            vmem((n_ep, 1, 128), F32), vmem((n_ep, 128), F32),
            vmem((width // share, share, 128), BF16), vmem((n_ep, share, 128), BF16),
            dma((6,)),
            dma, dma, dma, dma((nz,)), dma, dma((nz,)), dma, dma((nz,)), dma, dma, dma((nz,)),
            dma, dma((nz,)),
            dma, dma((chunks,)), dma, dma((chunks,)), dma, dma((chunks,)), dma, dma((chunks,)),
            dma, dma((chunks,)),
            dma, dma((chunks,)), dma, dma, dma, dma, dma, dma,
        ]
        shape = jax.ShapeDtypeStruct
        results = pl.pallas_call(
            lambda *refs: kernel(n_ep, n_tp, hidden, *refs),
            out_shape=(
                shape((rows, cols), BF16), shape((2, rows), F32), shape((share, experts), F32),
                shape((hidden, width), BF16), shape((hidden, width), BF16),
                shape((hidden, width), BF16),
            ),
            in_specs=[any_, whole, any_, any_, any_, any_, any_],
            out_specs=(whole,) * 6,
            scratch_shapes=scratch,
            compiler_params=pltpu.CompilerParams(
                collective_id=0, has_side_effects=True, vmem_limit_bytes=VMEM_LIMIT
            ),
            name="moe_backward",
        )(
            *(
                pltpu.with_memory_space_constraint(a, pltpu.HBM)
                for a in (
                    tokens, routes.T, router_matrix.T, cotangent, jnp.swapaxes(gate_proj, 1, 2),
                    jnp.swapaxes(up_proj, 1, 2), down_proj,
                )
            )
        )
        token_grad, mixing, router_grad, gate_grad, up_grad, down_grad = pl.pallas_call(
            hand_over,
            out_shape=tuple(shape(r.shape, r.dtype) for r in results),
            in_specs=[whole] * 6,
            out_specs=(any_,) * 6,
            scratch_shapes=[dma((6,))],
            compiler_params=pltpu.CompilerParams(vmem_limit_bytes=2**20),
            name="hand_over",
        )(*results)
        return (
            token_grad, mixing.T, router_grad, gate_grad.T[None], up_grad.T[None], down_grad[None]
        )

    return jax.shard_map(
        local,
        mesh=mesh,
        in_specs=(
            P("ep", None), P("ep", None), P(), P("ep", "tp"),
            P("ep", None, "tp"), P("ep", None, "tp"), P("ep", "tp", None),
        ),
        out_specs=(
            P("ep", "tp"), P("ep", None), P(("ep", "tp"), None),
            P("ep", None, "tp"), P("ep", None, "tp"), P("ep", "tp", None),
        ),
        check_vma=False,
    )
```

time: 128 us -> 91.7 us (0.72)
  local copies, waits for them, and re-layouts: 21.8 us -> 0 us
  Pallas kernels: 105 us -> 89.7 us
    unnamed x18 -> x0, local copies, waits for them, and re-layouts: 21.8 us -> none
    pallas_call x1 -> x2, Pallas kernels: 105 us -> 89.7 us  [the longest x1 87.1 us: local(): pl.pallas_call(lambda *refs: kernel(n_ep, n_tp, hidden, *refs), out_shape...]
where the time goes in v2:
time: 91.7 us; the launch traced here: 90.5 us
  Pallas kernels  89.7 us (98%)
    pallas_call x1, Pallas kernels, local(): pl.pallas_call(lambda *refs: kernel(n_ep, n_tp, hidden, *refs), out_shape...  87.1 us
    pallas_call x1, Pallas kernels, local(): pl.pallas_call(hand_over, out_shape=tuple((shape(r.shape, r.dtype) for r...  2.54 us

profile of v2, /device:TPU:8, one launch (start us, length us, event | category | flops | bytes accessed | tf_op | source)
XLA Modules:
  0.0 90.5 jit_solution(1337065014961298364)
XLA Ops:
  0.6 87.1 %moe_backward.1 = (bf16[256,256]{1,0:T(8,128)(2,1)S(1)}, f32[2,256]{1,0:T(2,128)S(1)}, f32[8,32]{1,0:T(8,128)S(1)}, bf16[448,2048]{1,0:T(8,128)(2,1)S(1)}, bf16[...) custom-call(bf16[256,2048]{1,0:T(8,128)(2,1)} %refs_0_.1, s32[2,256]{1,0:T(2,128)} %bitcast.15, ...), custom_call_target="tpu_custom_call" | custom-call | tf_op jit(solution)/shard_map/moe_backward/pallas_call | solution.py:556
  87.8 2.5 %hand_over.1 = (bf16[256,256]{1,0:T(8,128)(2,1)}, f32[2,256]{1,0:T(2,128)}, f32[8,32]{1,0:T(8,128)}, bf16[448,2048]{1,0:T(8,128)(2,1)}, bf16[448,2048]{1,0:T(8,128)(2,1)}, /*index=5*/bf16[448,2048]{1,0:T(8,128)(2,1)}) custom-call(bf16[256,256]{1,0:T(8,128)(2,1)S(1)} %get-tuple-element.18.refs_0_, f32[2,256]{1,0:T(2,128)S(1)} %get-tuple-element.19.refs_1_, ...), custom_call_target="tpu_custom_call" | custom-call | tf_op jit(solution)/shard_map/hand_over/pallas_call | solution.py:579

commit v3 on v2

--- a/solution.py
+++ b/solution.py
@@ -97,11 +97,6 @@
             if dz or dx:
                 ep_peers.append((g, ring(z, -dz, nz), ring(x, dx, NX)))
 
-    barrier = pltpu.get_barrier_semaphore()
-    for _, pz, px in ep_peers:
-        pl.semaphore_signal(barrier, inc=1, device_id=(pz * NX + px, tp), device_id_type=MESH)
-    for d in range(1, n_tp):
-        pl.semaphore_signal(barrier, inc=1, device_id=(ep, ring(tp, d, n_tp)), device_id_type=MESH)
     loads = [
         pltpu.make_async_copy(a, b, lsem.at[k])
         for k, (a, b) in enumerate(
@@ -115,6 +110,11 @@
     ]
     for load in loads:
         load.start()
+    barrier = pltpu.get_barrier_semaphore()
+    for _, pz, px in ep_peers:
+        pl.semaphore_signal(barrier, inc=1, device_id=(pz * NX + px, tp), device_id_type=MESH)
+    for d in range(1, n_tp):
+        pl.semaphore_signal(barrier, inc=1, device_id=(ep, ring(tp, d, n_tp)), device_id_type=MESH)
     gap = jnp.zeros((hpad - hidden, width), BF16)
     w2[hidden:hpad, :] = gap
     w2[hpad + hidden :, :] = gap
@@ -183,13 +183,13 @@
         for load in loads[3:]:
             load.wait()
 
-        def flip(k, carry):
+        def flip_weights(k, carry):
             at = pl.ds(pl.multiple_of(k * cols, cols), cols)
             w2_t[at, :] = w2[:, at].T
             wd_t[at, :] = wd[:, at].T
             return carry
 
-        lax.fori_loop(0, n_tp, flip, 0)
+        lax.fori_loop(0, n_tp, flip_weights, 0)
 
     def to_partner(share, g):
         piece = gathered.at[share, g]
@@ -280,8 +280,11 @@
     def turn(q):
         eye = iota((group, group), 0) == iota((group, group), 1)
         for m in range(2):
-            column = mix_col[m * group : (m + 1) * group, :]
-            mix_row[2 * q + m] = jnp.sum(jnp.where(eye, column, 0.0), axis=0, keepdims=True)
+            part = mix_col[m * group : (m + 1) * group, :]
+            mix_row[2 * q + m] = jnp.sum(jnp.where(eye, part, 0.0), axis=0, keepdims=True)
+
+    @phase
+    def flip(q):
         hid_t[:, q * chunk : (q + 1) * chunk] = hid[...].T
         gu_t[:, q * chunk : (q + 1) * chunk] = gu[q * chunk : (q + 1) * chunk, :].T
 
@@ -396,17 +399,20 @@
             rs_bc(q - 1)
         backward(q)
         element(q)
-        poll(2 * q + 4)
+        if q < last - 1:
+            poll(2 * q + 4)
         term(q)
         rs_a(q)
+        if q == last - 1:
+            poll(2 * q + 4)
+        turn(q)
+        mix_out(q)
+        flip(q)
         if q >= 1:
+            mix_home(q - 1)
             rs_de(q - 1)
         if q >= 2:
             rs_fg(q - 2)
-        turn(q)
-        mix_out(q)
-        if q >= 1:
-            mix_home(q - 1)
 
     ready(last)
     forward(last)
@@ -417,15 +423,17 @@
     mix_out(last)
     term(last)
     rs_a(last)
+    flip(last)
     rs_de(last - 1)
+    rs_bc(last)
+    rs_fg(last - 2)
     mix_home(last - 1)
+    grads(0, 3)
     mix_home(last)
-    rs_fg(last - 2)
-    rs_bc(last)
-    grads(0, 2)
+    grads(3, 5)
     rs_fg(last - 1)
-    grads(2, 3)
     rs_de(last)
+    grads(5, 6)
 
     with jax.named_scope("mix_wait"):
         wait_in(mix_in.at[pl.ds(0, n_ep - 1)], mx_s, mx_r)
@@ -464,9 +472,8 @@
     rin[ep] = rparts[ep * n_tp + tp]
     router_cols = router[:, pl.ds(pl.multiple_of(tp * cols, cols), cols)]
     path = dot(rg_hi[:, :experts], router_cols) + dot(rg_lo[:, :experts], router_cols)
-    grads(3, 5)
     rs_fg(last)
-    grads(5, n_tp)
+    grads(6, n_tp)
 
     with jax.named_scope("ret_wait"):
         wait_in(ret_in.at[pl.ds(0, n_ep - 1)], ret_s, ret_r)

time: 91.7 us -> 91.5 us (level); the launches traced: 90.5 us -> 91.4 us
  no operation moved by 1% of the time
where the time goes in v3:
time: 91.5 us; the launch traced here: 91.4 us
  Pallas kernels  90.6 us (99%)
    pallas_call x1, Pallas kernels, local(): pl.pallas_call(lambda *refs: kernel(n_ep, n_tp, hidden, *refs), out_shape...  88 us
    pallas_call x1, Pallas kernels, local(): pl.pallas_call(hand_over, out_shape=tuple((shape(r.shape, r.dtype) for r...  2.54 us

profile of v3, /device:TPU:8, one launch (start us, length us, event | category | flops | bytes accessed | tf_op | source)
XLA Modules:
  0.0 91.4 jit_solution(13682703195848910710)
XLA Ops:
  0.6 88.0 %moe_backward.1 = (bf16[256,256]{1,0:T(8,128)(2,1)S(1)}, f32[2,256]{1,0:T(2,128)S(1)}, f32[8,32]{1,0:T(8,128)S(1)}, bf16[448,2048]{1,0:T(8,128)(2,1)S(1)}, bf16[...) custom-call(bf16[256,2048]{1,0:T(8,128)(2,1)} %refs_0_.1, s32[2,256]{1,0:T(2,128)} %bitcast.15, ...), custom_call_target="tpu_custom_call" | custom-call | tf_op jit(solution)/shard_map/moe_backward/pallas_call | solution.py:563
  88.7 2.5 %hand_over.1 = (bf16[256,256]{1,0:T(8,128)(2,1)}, f32[2,256]{1,0:T(2,128)}, f32[8,32]{1,0:T(8,128)}, bf16[448,2048]{1,0:T(8,128)(2,1)}, bf16[448,2048]{1,0:T(8,128)(2,1)}, /*index=5*/bf16[448,2048]{1,0:T(8,128)(2,1)}) custom-call(bf16[256,256]{1,0:T(8,128)(2,1)S(1)} %get-tuple-element.18.refs_0_, f32[2,256]{1,0:T(2,128)S(1)} %get-tuple-element.19.refs_1_, ...), custom_call_target="tpu_custom_call" | custom-call | tf_op jit(solution)/shard_map/hand_over/pallas_call | solution.py:586
